TPU v7x, 512 devices: a whole 4x4x16 slice. The times are simulated.
512 devices in a mesh: fs: 64 (over z, y), tp: 8 (over x, core).
Axes of the slice: x: 4, y: 4, z: 16, core: 2. Of those that a mesh axis runs over, the one named last changes fastest.
Arguments:
- tokens: bfloat16 [16384, 2048], P('fs', 'tp'), may hold values from -16 to 16, as said below
- mix_gain: bfloat16 [2048], P('tp'), may hold values from 0.099609375 to 1.8984375
- query_weight: bfloat16 [2048, 512], P('fs', 'tp'), may hold values from -0.125 to 0.125
- key_weight: bfloat16 [2048, 512], P('fs', 'tp'), may hold values from -0.125 to 0.125
- value_weight: bfloat16 [2048, 1024], P('fs', 'tp'), may hold values from -0.125 to 0.125
- output_gate_weight: bfloat16 [2048, 1024], P('fs', 'tp'), may hold values from -0.125 to 0.125
- out_weight: bfloat16 [1024, 2048], P('tp', 'fs'), may hold values from -0.1875 to 0.1875
- head_rates: float32 [8], P('tp'), may hold values from 0 to 1, as said below
- block_scale: float32 [128], P('fs'), may hold values from 0.5 to 2
- ffn_gain: bfloat16 [2048], P('tp'), may hold values from 0.099609375 to 1.8984375
- ff_gate: bfloat16 [2048, 5632], P('fs', 'tp'), may hold values from -0.125 to 0.125
- ff_up: bfloat16 [2048, 5632], P('fs', 'tp'), may hold values from -0.125 to 0.125
- ff_down: bfloat16 [5632, 2048], P('tp', 'fs'), may hold values from -0.078125 to 0.078125
- final_gain: bfloat16 [2048], P('tp'), may hold values from 0.099609375 to 1.8984375
Outputs:
- layer_out: bfloat16 [16384, 2048], P('fs', 'tp')
Inputs may be any that keep to these rules, and one draw needn't show every extreme that they name: `tokens`: column blocks of the activations have different scales. `head_rates`: positive rates.
All inputs are finite; a program needn't handle non-finite values.
Results may differ from a plain program's by a relative error of at most 0.014.
Values may be sent and summed in bfloat16 or wider, within the bound.
A program may use at most 64 MiB of HBM per device.

v0:
```python
import jax
import jax.numpy as jnp
from jax import lax
from jax.sharding import Mesh
from jax.sharding import PartitionSpec as P

D = 2048
DK = 64
DV = 128
BLK = 128
SEQ_LEN = 256
FS = ("fs_0", "fs_1")


EPS = 1e-06
THETA = 10000.0


def gather_turned(arrays, axis, dims):
    turned = [jnp.moveaxis(a, dim, 0) for a, dim in zip(arrays, dims)]
    both = jnp.concatenate([t.reshape(len(t), -1) for t in turned], axis=1)
    filled, at, outs = (lax.all_gather(both, axis, axis=0, tiled=True), 0, [])
    for t, dim in zip(turned, dims):
        share = filled[:, at : at + t[0].size].reshape(-1, *t.shape[1:])
        outs.append(jnp.moveaxis(share, 0, dim))
        at += t[0].size
    return tuple(outs)


def sent_together(arrays, axis, dim, along):
    widths = [a.shape[along] for a in arrays]
    both = jnp.concatenate(arrays, axis=along)
    filled = lax.all_gather(both, axis, axis=dim, tiled=True)
    return tuple(jnp.split(filled, [sum(widths[:k]) for k in range(1, len(widths))], axis=along))


def laid_out(tiles, dim):
    lengths = list(tiles.shape[1:])
    lengths[dim] *= tiles.shape[0]
    return jnp.moveaxis(tiles, 0, dim).reshape(lengths)


def copy_for_each(shard, axis):
    size = lax.axis_size(axis)
    return lax.all_to_all(
        jnp.broadcast_to(shard[None], (size, *shard.shape)), axis, 0, 0, tiled=True
    )


def gather_directly(shard, axis, dim):
    return laid_out(copy_for_each(shard, axis), dim)


def gathered_by_axis(shard, axes, dim):
    filled = shard
    for number in range(len(axes) - 1, -1, -1):
        filled = lax.all_gather(filled, axes[number], axis=dim, tiled=True)
    return filled


def in_blocks(shard, dim, size):
    lengths = shard.shape
    tiles = shard.reshape(*lengths[:dim], size, lengths[dim] // size, *lengths[dim + 1 :])
    return jnp.moveaxis(tiles, dim, 0)


def sent_and_summed(shard, axis, dim):
    size = lax.axis_size(axis)
    tiles = lax.all_to_all(in_blocks(shard, dim, size), axis, 0, 0, tiled=True)
    return jnp.sum(tiles.astype(jnp.float32), axis=0)


def of_everyone(shard, axis):
    return copy_for_each(shard, axis).sum(axis=0)


def rms_norm(values, gain):
    scale = lax.rsqrt(jnp.mean(values * values, axis=-1, keepdims=True) + EPS)
    return values * scale * gain.astype(jnp.float32)


def rotate(values, positions):
    half = values.shape[-1] // 2
    inverse = THETA ** (-jnp.arange(half, dtype=jnp.float32) / half)
    angle = positions.astype(jnp.float32)[:, None] * inverse
    cosine = jnp.cos(angle)[:, None, :]
    sine = jnp.sin(angle)[:, None, :]
    first = values[..., :half]
    second = values[..., half:]
    return jnp.concatenate(
        [first * cosine - second * sine, second * cosine + first * sine], axis=-1
    )


def retain(query, key, value, rates, scales):
    rows, heads_here, width_k = query.shape
    width_v = value.shape[-1]
    nblk = rows // BLK
    hi = lax.Precision.HIGHEST
    qblk = query.astype(jnp.float32).reshape(nblk, BLK, heads_here, width_k)
    kblk = key.astype(jnp.float32).reshape(nblk, BLK, heads_here, width_k)
    vblk = value.astype(jnp.float32).reshape(nblk, BLK, heads_here, width_v)
    logdec = -rates[None, :] * scales[:, None]
    steps = jnp.arange(BLK, dtype=jnp.float32)
    offset = steps[:, None] - steps[None, :]
    causal = offset >= 0
    inside = jnp.where(
        causal[None, None],
        jnp.exp(logdec[:, :, None, None] * jnp.where(causal, offset, 0.0)[None, None]),
        0.0,
    )
    scores = jnp.einsum("nchd,nmhd->nhcm", qblk, kblk, precision=hi) * inside
    inner = jnp.einsum("nhcm,nmhe->nche", scores, vblk, precision=hi)
    zeta = jnp.exp(logdec[:, :, None] * (BLK - 1.0 - steps)[None, None, :])
    kv_block = jnp.einsum(
        "nchd,nche->nhde", kblk * jnp.transpose(zeta, (0, 2, 1))[..., None], vblk, precision=hi
    )
    hold = jnp.exp(logdec * BLK)
    per_seq = SEQ_LEN // BLK
    fresh = (jnp.arange(nblk, dtype=jnp.int32) % per_seq == 0).astype(jnp.float32)

    def advance(state, inputs):
        kv_now, hold_now, fresh_now = inputs
        before = state * (1.0 - fresh_now)
        return (before * hold_now[:, None, None] + kv_now, before)

    start = jnp.zeros((heads_here, width_k, width_v), jnp.float32)
    _, before = lax.scan(advance, start, (kv_block, hold, fresh))
    xi = jnp.exp(logdec[:, :, None] * (steps + 1.0)[None, None, :])
    cross = jnp.einsum(
        "nchd,nhde->nche", qblk * jnp.transpose(xi, (0, 2, 1))[..., None], before, precision=hi
    )
    total = inner + cross
    total = total * lax.rsqrt(jnp.mean(total * total, axis=-1, keepdims=True) + EPS)
    return total.reshape(rows, heads_here * width_v)


def body(
    tokens,
    mix_gain,
    query_weight,
    key_weight,
    value_weight,
    output_gate_weight,
    out_weight,
    head_rates,
    block_scale,
    ffn_gain,
    ff_gate,
    ff_up,
    ff_down,
    final_gain,
):
    rows = tokens.shape[0]
    heads_here = head_rates.shape[0]
    groups = lax.axis_size("tp")
    positions = jnp.arange(rows, dtype=jnp.int32) % SEQ_LEN
    whole, gain_whole = gather_turned((tokens, mix_gain), "tp", (1, 0))
    normed = rms_norm(whole.astype(jnp.float32), gain_whole).astype(jnp.bfloat16)
    collected = sent_together(
        (query_weight, key_weight, value_weight, output_gate_weight), FS, 0, 1
    )
    qproj, kproj, vproj, gproj = tuple(
        (jnp.dot(normed, weight, preferred_element_type=jnp.float32) for weight in collected)
    )
    query = rotate(qproj.reshape(rows, heads_here, DK), positions).astype(jnp.bfloat16)
    key = (rotate(kproj.reshape(rows, heads_here, DK), positions) * DK ** (-0.5)).astype(
        jnp.bfloat16
    )
    value = vproj.astype(jnp.bfloat16).reshape(rows, heads_here, DV)
    normret = retain(query, key, value, head_rates, block_scale)
    gated = (normret * jax.nn.silu(gproj)).astype(jnp.bfloat16)
    all_heads = gather_directly(gated, "tp", 1)
    head_rows = gathered_by_axis(out_weight, FS, 1)
    feature_block = lax.all_to_all(head_rows, "tp", split_axis=1, concat_axis=0, tiled=True)
    width = all_heads.shape[1] // groups
    left = all_heads.reshape(rows, groups, width)
    right = feature_block.reshape(groups, width, feature_block.shape[1])
    partial_sums = jnp.einsum(
        "rng,nge->nre", left, right, preferred_element_type=jnp.float32
    ).astype(jnp.bfloat16)
    mix = jnp.sum(partial_sums.astype(jnp.float32), axis=0)
    resid = (tokens.astype(jnp.float32) + mix).astype(jnp.bfloat16)
    whole2, gain2 = gather_turned((resid, ffn_gain), "tp", (1, 0))
    normed2 = rms_norm(whole2.astype(jnp.float32), gain2).astype(jnp.bfloat16)
    gate_rows, up_rows = sent_together((ff_gate, ff_up), FS, 0, 1)
    gate_part = jnp.dot(normed2, gate_rows, preferred_element_type=jnp.float32)
    up_part = jnp.dot(normed2, up_rows, preferred_element_type=jnp.float32)
    hidden = (jax.nn.silu(gate_part) * up_part).astype(jnp.bfloat16)
    down_terms = jnp.dot(
        hidden, gathered_by_axis(ff_down, FS, 1), preferred_element_type=jnp.float32
    )
    ffn = sent_and_summed(down_terms.astype(jnp.bfloat16), "tp", 1)
    total = resid.astype(jnp.float32) + ffn
    squares = of_everyone(jnp.sum(total * total, axis=-1, keepdims=True), "tp")
    scale = lax.rsqrt(squares / D + EPS)
    return (total * scale * final_gain.astype(jnp.float32)).astype(jnp.bfloat16)


def solution(mesh):
    finer = Mesh(mesh.devices.reshape(16, 4, mesh.shape["tp"]), ("fs_0", "fs_1", "tp"))
    return jax.shard_map(
        body,
        mesh=finer,
        in_specs=(
            P(FS, "tp"),
            P("tp"),
            P(FS, "tp"),
            P(FS, "tp"),
            P(FS, "tp"),
            P(FS, "tp"),
            P("tp", FS),
            P("tp"),
            P(FS),
            P("tp"),
            P(FS, "tp"),
            P(FS, "tp"),
            P("tp", FS),
            P("tp"),
        ),
        out_specs=P(FS, "tp"),
        check_vma=False,
    )
```

profile of v0, /device:TPU:1, one launch (start us, length us, event | category | flops | bytes accessed | tf_op | source)
XLA Modules:
  0.0 515.7 jit_solution(17452584656318330392)
XLA Ops:
  6.5 0.7 reshape.400
  7.2 1.6 pad_maximum_fusion
  8.9 1.4 pad_maximum_fusion.3
  10.3 10.6 %all_gather.26 = bf16[128,128]{0,1:T(8,128)(2,1)S(1)} all-gather(bf16[128,32]{0,1:T(8,128)(2,1)} %param.22), channel_id=1, replica_groups=mesh['fs_0'=16,'fs_1'=4,'tp'=8] {'fs_1'}, dimensions={1}, use_global_device_ids=true | all-gather | bytes 40960 | tf_op jit(solution)/shard_map/all_gather | solution.py:57
  20.9 31.9 %all_gather.27 = bf16[128,2048]{0,1:T(8,128)(2,1)S(1)} all-gather(bf16[128,128]{0,1:T(8,128)(2,1)S(1)} %all_gather.26), channel_id=1, replica_groups=mesh['fs_0'=16,'fs_1'=4,'tp'=8] {'fs_0'}, dimensions={1}, use_global_device_ids=true | all-gather | bytes 557056 | tf_op jit(solution)/shard_map/all_gather | solution.py:57
  52.8 1.0 copy.31
  53.8 14.1 %all-to-all-start.1 = ((bf16[128,8,256]{2,0,1:T(8,128)(2,1)}), bf16[128,8,256]{2,0,1:T(8,128)(2,1)S(1)}, u32[]{:S(2)}, u32[]{:S(2)}) async-start(bf16[128,8,256]{2,0,1:T(8,128)(2,1)} %copy.31), calls=%async_computation.1 | async-start | bytes 1048576 | tf_op jit(solution)/shard_map/all_to_all | solution.py:175
  68.9 1.6 fusion.4
  70.5 0.8 slice_convert_fusion.1
  71.2 109.0 %all-gather.8.cloned.1.call-done = bf16[2048,384]{1,0:T(8,128)(2,1)} async-done(((bf16[32,384]{1,0:T(8,128)(2,1)}), bf16[2048,384]{1,0:T(8,128)(2,1)}) %all-gather.8.cloned.1.call-update) | async-done | bytes 1572880 | tf_op jit(solution)/shard_map/all_gather | solution.py:33
  180.3 2.0 convolution_bitcast_fusion
  182.3 1.6 convolution_bitcast_fusion.1
  184.2 1.5 convolution_convert_fusion.2
  185.9 5.0 while.13
  192.1 1.6 fusion.35
  193.7 0.9 broadcast_in_dim.29
  194.6 15.1 %all-to-all-start = ((bf16[8,256,128]{2,1,0:T(8,128)(2,1)}), bf16[8,256,128]{2,1,0:T(8,128)(2,1)S(1)}, u32[]{:S(2)}, u32[]{:S(2)}) async-start(bf16[8,256,128]{2,1,0:T(8,128)(2,1)} %broadcast_in_dim.29), calls=%async_computation | async-start | bytes 1048576 | tf_op jit(solution)/shard_map/all_to_all | solution.py:45
  209.7 9.3 %all-to-all-done = bf16[8,256,128]{2,1,0:T(8,128)(2,1)S(1)} async-done(((bf16[8,256,128]{2,1,0:T(8,128)(2,1)}), bf16[8,256,128]{2,1,0:T(8,128)(2,1)S(1)}, u32[]{:S(2)}, u32[]{:S(2)}) %all-to-all-start) | async-done | bytes 524320 | tf_op jit(solution)/shard_map/all_to_all | solution.py:45
  219.5 0.7 pad_maximum_fusion.1
  220.3 0.7 pad_maximum_fusion.2
  221.1 10.0 %all_gather.30 = bf16[704,128]{0,1:T(8,128)(2,1)} all-gather(bf16[704,32]{0,1:T(8,128)(2,1)S(1)} %copy-done.5), channel_id=1, replica_groups=mesh['fs_0'=16,'fs_1'=4,'tp'=8] {'fs_1'}, dimensions={1}, use_global_device_ids=true | all-gather | bytes 225280 | tf_op jit(solution)/shard_map/all_gather | solution.py:57
  231.1 15.0 %all-gather.10.cloned.1.call-done = bf16[2048,257]{0,1:T(8,128)(2,1)} async-done(((bf16[256,257]{0,1:T(8,128)(2,1)}), bf16[2048,257]{0,1:T(8,128)(2,1)}) %all-gather.10.cloned.1.call-update) | async-done | bytes 1052688 | tf_op jit(solution)/shard_map/all_gather | solution.py:22
  246.0 1.5 fusion.7
  247.6 0.8 slice_convert_fusion
  248.3 142.7 %all-gather.12.cloned.1.call-done = bf16[2048,1408]{1,0:T(8,128)(2,1)} async-done(((bf16[32,1408]{1,0:T(8,128)(2,1)}), bf16[2048,1408]{1,0:T(8,128)(2,1)}) %all-gather.12.cloned.1.call-update) | async-done | bytes 5767184 | tf_op jit(solution)/shard_map/all_gather | solution.py:33
  391.0 3.7 fusion.2
  394.7 68.0 %all-gather.14.cloned.1.call-done = bf16[704,2048]{0,1:T(8,128)(2,1)} async-done(((bf16[704,128]{0,1:T(8,128)(2,1)}), bf16[704,2048]{0,1:T(8,128)(2,1)}) %all-gather.14.cloned.1.call-update) | async-done | bytes 2883600 | tf_op jit(solution)/shard_map/all_gather | solution.py:57
  462.7 7.2 %convolution_convert_fusion = bf16[256,2048]{1,0:T(8,128)(2,1)S(1)} fusion(bf16[704,2048]{0,1:T(8,128)(2,1)} %all-gather.14.cloned.1.call-done, bf16[2048,1408]{1,0:T(8,128)(2,1)} %all-gather.12.cloned.1.call-done, f32[256,704]{0,1:T(8,128)S(1)} %fusion.2, f32[2048]{0:T(1024)S(1)} %bitcast.82, f32[256]{0:T(256)S(1)} %add_rsqrt_fusion.1, ...), kind=kOutput, calls=%fused_computation.12 | convolution fusion | flops 1480097792 | bytes 9118720 | tf_op jit(solution)/shard_map/dot_general | solution.py:190
  470.1 28.6 %all_to_all.31 = bf16[8,256,256]{2,1,0:T(8,128)(2,1)S(1)} all-to-all(bf16[8,256,256]{2,1,0:T(8,128)(2,1)S(1)} %bitcast.70), channel_id=1, replica_groups=mesh['fs_0'=16,'fs_1'=4,'tp'=8] {'tp'}, dimensions={0} | all-to-all | bytes 2097152 | tf_op jit(solution)/shard_map/all_to_all | solution.py:69
  499.5 4.3 all-to-all-start.3
  503.8 4.6 all-to-all-done.3
  508.4 0.8 multiply_convert_fusion
  (75 shorter events, 7.1 us)
Async XLA Ops:
  6.5 62.2 %copy-start.6 = (f32[2]{0:T(128)S(1)}, f32[2]{0:T(128)}, u32[]{:S(2)}) copy-start(f32[2]{0:T(128)} %param.24) | copy-start | bytes 28
  6.5 62.3 %all-gather.6.cloned.1.call-start = ((), (), s32[]{:S(2)}) async-start(), calls=%async_computation.4 | async-start | bytes 1216512 | tf_op jit(solution)/shard_map/all_gather | solution.py:22
  8.8 171.5 %all-gather.8.cloned.1.call-start = ((), (), s32[]{:S(2)}) async-start(), calls=%async_computation.5 | async-start | bytes 1597440 | tf_op jit(solution)/shard_map/all_gather | solution.py:33
  53.8 139.9 %all-to-all-start.1 = ((bf16[128,8,256]{2,0,1:T(8,128)(2,1)}), bf16[128,8,256]{2,0,1:T(8,128)(2,1)S(1)}, u32[]{:S(2)}, u32[]{:S(2)}) async-start(bf16[128,8,256]{2,0,1:T(8,128)(2,1)} %copy.31), calls=%async_computation.1 | async-start | bytes 1048576 | tf_op jit(solution)/shard_map/all_to_all | solution.py:175
  68.9 113.5 %copy-start = (bf16[2048,257]{0,1:T(8,128)(2,1)S(1)}, bf16[2048,257]{0,1:T(8,128)(2,1)}, u32[]{:S(2)}) copy-start(bf16[2048,257]{0,1:T(8,128)(2,1)} %all-gather.6.cloned.1.call-done) | copy-start | bytes 3158020
  192.1 17.6 %copy-start.7 = (bf16[256]{0:T(256)(128)(2,1)S(1)}, bf16[256]{0:T(256)(128)(2,1)}, u32[]{:S(2)}) copy-start(bf16[256]{0:T(256)(128)(2,1)} %param.25) | copy-start | bytes 1540
  193.7 25.8 %copy-start.2 = (bf16[256,256]{1,0:T(8,128)(2,1)S(1)}, bf16[256,256]{1,0:T(8,128)(2,1)}, u32[]{:S(2)}) copy-start(bf16[256,256]{1,0:T(8,128)(2,1)} %param.16) | copy-start | bytes 393220
  193.7 26.6 %copy-start.3 = (bf16[32,704]{1,0:T(8,128)(2,1)S(1)}, bf16[32,704]{1,0:T(8,128)(2,1)}, u32[]{:S(2)}) copy-start(bf16[32,704]{1,0:T(8,128)(2,1)} %param.27) | copy-start | bytes 135172
  193.7 26.6 %copy-start.4 = (bf16[32,704]{1,0:T(8,128)(2,1)S(1)}, bf16[32,704]{1,0:T(8,128)(2,1)}, u32[]{:S(2)}) copy-start(bf16[32,704]{1,0:T(8,128)(2,1)} %param.26) | copy-start | bytes 135172
  193.7 27.3 %copy-start.5 = (bf16[704,32]{0,1:T(8,128)(2,1)S(1)}, bf16[704,32]{0,1:T(8,128)(2,1)}, u32[]{:S(2)}) copy-start(bf16[704,32]{0,1:T(8,128)(2,1)} %param.28) | copy-start | bytes 135172
  194.6 24.4 %all-to-all-start = ((bf16[8,256,128]{2,1,0:T(8,128)(2,1)}), bf16[8,256,128]{2,1,0:T(8,128)(2,1)S(1)}, u32[]{:S(2)}, u32[]{:S(2)}) async-start(bf16[8,256,128]{2,1,0:T(8,128)(2,1)} %broadcast_in_dim.29), calls=%async_computation | async-start | bytes 1048576 | tf_op jit(solution)/shard_map/all_to_all | solution.py:45
  209.7 36.4 %all-gather.10.cloned.1.call-start = ((), (), s32[]{:S(2)}) async-start(), calls=%async_computation.6 | async-start | bytes 1216512 | tf_op jit(solution)/shard_map/all_gather | solution.py:22
  220.2 170.8 %all-gather.12.cloned.1.call-start = ((), (), s32[]{:S(2)}) async-start(), calls=%async_computation.7 | async-start | bytes 5857280 | tf_op jit(solution)/shard_map/all_gather | solution.py:33
  221.0 241.7 %all-gather.14.cloned.1.call-start = ((), (), s32[]{:S(2)}) async-start(), calls=%async_computation.8 | async-start | bytes 3342336 | tf_op jit(solution)/shard_map/all_gather | solution.py:57
  391.0 71.7 %copy-start.1 = (bf16[2048,257]{0,1:T(8,128)(2,1)S(1)}, bf16[2048,257]{0,1:T(8,128)(2,1)}, u32[]{:S(2)}) copy-start(bf16[2048,257]{0,1:T(8,128)(2,1)} %all-gather.10.cloned.1.call-done) | copy-start | bytes 3158020
  470.0 33.7 %copy-start.8 = (bf16[256]{0:T(256)(128)(2,1)S(1)}, bf16[256]{0:T(256)(128)(2,1)}, u32[]{:S(2)}) copy-start(bf16[256]{0:T(256)(128)(2,1)} %param.29) | copy-start | bytes 1540
  499.5 8.9 %all-to-all-start.3 = ((f32[8,256,1]{1,2,0:T(1,128)}), f32[8,256,1]{1,2,0:T(1,128)S(1)}, u32[]{:S(2)}, u32[]{:S(2)}) async-start(f32[8,256,1]{1,2,0:T(1,128)} %broadcast_in_dim.30), calls=%async_computation.3 | async-start | bytes 16384 | tf_op jit(solution)/shard_map/all_to_all | solution.py:45
Sparse Core Ops, SparseCore 0:
  9.4 36.6 all-gather.5
  49.1 131.1 all-gather.7
  220.3 25.6 all-gather.9
  248.8 142.1 all-gather.11
  392.9 69.7 all-gather.13
where the time goes:
time: 517 us; the launch traced here: 516 us
  waiting for transfers between devices  349 us (68%)
  blocking collectives  81 us (16%)
  starting transfers between devices  33.6 us (6%)
  matrix products  19.1 us (4%)
  between operations  14.1 us (3%)
  other arithmetic  12 us (2%)
  local copies, waits for them, and re-layouts  5.72 us (1%)
    all_gather x2, waiting for transfers between devices, sent_together(): filled = lax.all_gather(both, axis, axis=dim, tiled=True)  252 us
    all_gather x1, waiting for transfers between devices, gathered_by_axis(): filled = lax.all_gather(filled, axes[number], axis=dim, tiled=True)  68 us
    all_gather x3, blocking collectives, gathered_by_axis(): filled = lax.all_gather(filled, axes[number], axis=dim, tiled=True)  52.5 us
    all_to_all x1, blocking collectives, sent_and_summed(): tiles = lax.all_to_all(in_blocks(shard, dim, size), axis, 0, 0, tiled=True)  28.6 us
    all_to_all x2, starting transfers between devices, copy_for_each(): lax.all_to_all(jnp.broadcast_to(shard[None], (size, *shard.shape)), axis,...  19.4 us
    all_gather x2, waiting for transfers between devices, gather_turned(): filled, at, outs = (lax.all_gather(both, axis, axis=0, tiled=True), 0, [])  15 us
    all_to_all x1, starting transfers between devices, body(): lax.all_to_all(head_rows, 'tp', split_axis=1, concat_axis=0, tiled=True)  14.1 us
    all_to_all x2, waiting for transfers between devices, copy_for_each(): lax.all_to_all(jnp.broadcast_to(shard[None], (size, *shard.shape)), axis,...  14 us
  transfers between devices with their start and end apart: 8, of which 6 were waited for; matrix products, arithmetic and copies ran while one was open for 5% of the time, Pallas kernels for 0%

commit v1 on v0

v1 whole, which is shorter than its diff:
```python
import jax
import jax.numpy as jnp
import numpy as np
from jax import lax
from jax.experimental import pallas as pl
from jax.experimental.pallas import tpu as pltpu
from jax.sharding import PartitionSpec as P

MESH = pl.DeviceIdType.MESH
F32 = jnp.float32
BF16 = jnp.bfloat16
EPS = 1e-06
THETA = 10000.0
D = 2048
DK = 64
BLK = 128
SEQ = 256
Z, Y, X, C = 16, 4, 4, 2
HID = 176
NT = (((1,), (1,)), ((), ()))
N_SEND, N_RECV = 110, 170


def dot(a, b):
    return jnp.dot(a, b, preferred_element_type=F32)


def dot_nt(a, b):
    return lax.dot_general(a, b, NT, preferred_element_type=F32)


def iota(shape, dim):
    return lax.broadcasted_iota(jnp.int32, shape, dim)


def copy_to(src, dst, send, recv, where):
    return pltpu.make_async_remote_copy(
        src_ref=src, dst_ref=dst, send_sem=send, recv_sem=recv, device_id=where, device_id_type=MESH
    )


def wait_bytes(ref, sem):
    pltpu.make_async_copy(ref, ref, sem).wait()


def kernel(
    tok, mix_gain, qw, kw, vw, gw, ow, rates, scales, ffn_gain, ffg, ffu, ffd, fin, cos, sin,
    out,
    wq, slab, a2a, ffw, xt, xn, wo, gat, res, x2, part, sib, r1, r2, r3, r4, stat, stats,
    ssem, rsem, zsend, ysend, fsend, yshare,
):
    fs, tp = lax.axis_index("fs"), lax.axis_index("tp")
    z, y = fs // Y, fs % Y
    x, c = tp // C, tp % C
    o = 1 - c
    zr, zl = (z + 1) % Z, (z + Z - 1) % Z
    yp, y2, ym = (y + 1) % Y, (y + 2) % Y, (y + 3) % Y
    xp, xo, xm = (x + 1) % X, (x + 2) % X, (x + 3) % X

    def at(zz=z, yy=y, xx=x, cc=c):
        return (zz * Y + yy, xx * C + cc)

    used = [0, 0]
    pending = []

    def fresh():
        used[1] += 1
        return rsem.at[used[1] - 1]

    def send(src, dst, recv, where):
        used[0] += 1
        copy = copy_to(src, dst, ssem.at[used[0] - 1], recv, where)
        copy.start()
        pending.append(copy)
        return copy

    class Ring4:
        def __init__(self, slab_of, me, prev, nxt, to_prev, to_next):
            self.slab, self.me, self.prev, self.nxt = slab_of, me, prev, nxt
            self.to_prev, self.to_next = to_prev, to_next
            self.sems = [fresh() for _ in range(4)]

        def start(self):
            s = self.slab(self.me)
            self.a = send(s, s, self.sems[0], self.to_next)
            self.b = send(s, s, self.sems[1], self.to_prev)

        def relay(self):
            self.a.wait_recv()
            s = self.slab(self.prev, 0)
            self.d = send(s, s, self.sems[2], self.to_next)
            self.b.wait_recv()
            s = self.slab(self.nxt, 1)
            self.e = send(s, s, self.sems[3], self.to_prev)

        def finish(self):
            self.d.wait_recv()
            self.e.wait_recv()

    row0 = pl.multiple_of(z * (Y * 32) + y * 32, 32)
    e0 = (iota((64, 128), 0) == iota((64, 128), 1)).astype(BF16)
    e1 = (iota((64, 128), 0) + 64 == iota((64, 128), 1)).astype(BF16)
    i32 = (iota((32, 32), 0) == iota((32, 32), 1)).astype(BF16)
    wq[pl.ds(row0, 32), 0:128] = (dot(qw[...], e0) + dot(kw[...], e1)).astype(BF16)
    wq[pl.ds(row0, 32), 128:256] = vw[...]
    wq[pl.ds(row0, 32), 256:384] = gw[...]
    wq[pl.ds(row0, 32), 384:512] = dot_nt(i32, ow[...]).astype(BF16)
    xt[c, x, 0:256, :] = tok[...]
    xt[c, x, 256:272, :] = jnp.concatenate(
        [jnp.broadcast_to(mix_gain[...], (8, 256)), jnp.broadcast_to(ffn_gain[...], (8, 256))], axis=0
    )
    gt = ffg[...].astype(F32)
    ut = ffu[...].astype(F32)
    zero = jnp.zeros((32, 704), F32)
    tall = jnp.concatenate([gt, ut, zero, zero], axis=0)
    tall = jnp.concatenate([tall, jnp.zeros((128, 64), F32)], axis=1)
    turned = tall.T
    ed = (iota((32, 128), 0) + 64 == iota((32, 128), 1)).astype(BF16)
    slab[...] = (turned[0:704, :] + dot(ffd[...], ed)).astype(BF16)

    barrier = pltpu.get_barrier_semaphore()
    partners = [at(zz=zr), at(zz=zl), at(yy=yp), at(yy=y2), at(yy=ym)]
    partners += [at(xx=xx, cc=cc) for xx in (x, xp, xo, xm) for cc in (c, o)][1:]
    for who in partners:
        pl.semaphore_signal(barrier, inc=1, device_id=who, device_id_type=MESH)
    pl.semaphore_wait(barrier, len(partners))

    def wblk(zz, yy):
        return wq.at[pl.ds(pl.multiple_of(zz * (Y * 32) + yy * 32, 32), 32), :]

    left_sem = [fresh() for _ in range(8)]
    right_sem = [fresh() for _ in range(7)]
    yleft = [fresh() for _ in range(9)]
    yright = [fresh() for _ in range(7)]

    def z_send(zz, sem, where):
        copy_to(wblk(zz, y), wblk(zz, y), zsend, sem, where).start()

    def y_send(zz, yy, sem, where):
        copy_to(wblk(zz, yy), wblk(zz, yy), ysend, sem, where).start()

    def serve_w(s):
        if s == 0:
            z_send(z, left_sem[0], at(zz=zr))
            z_send(z, right_sem[0], at(zz=zl))
            y_send(z, y, yleft[0], at(yy=yp))
            y_send(z, y, yshare.at[1], at(yy=ym))
            return
        if s <= 8:
            zz = (z + Z - s) % Z
            copy_to(wblk(zz, y), wblk(zz, y), zsend, left_sem[s - 1], at(zz=zr)).wait_recv()
            if s < 8:
                z_send(zz, left_sem[s], at(zz=zr))
            y_send(zz, y, yleft[s], at(yy=yp))
            y_send(zz, y, yshare.at[1], at(yy=ym))
        if s <= 7:
            zz = (z + s) % Z
            copy_to(wblk(zz, y), wblk(zz, y), zsend, right_sem[s - 1], at(zz=zl)).wait_recv()
            if s < 7:
                z_send(zz, right_sem[s], at(zz=zl))
            y_send(zz, y, yright[s - 1], at(yy=ym))
            y_send(zz, y, yshare.at[0], at(yy=yp))

    def relay_y(s):
        zz = (z + Z - s) % Z
        copy_to(wblk(zz, ym), wblk(zz, ym), ysend, yleft[s], at(yy=yp)).wait_recv()
        y_send(zz, ym, yshare.at[2], at(yy=yp))
        if 1 <= s <= 7:
            zz = (z + s) % Z
            copy_to(wblk(zz, yp), wblk(zz, yp), ysend, yright[s - 1], at(yy=ym)).wait_recv()
            y_send(zz, yp, yshare.at[3], at(yy=ym))

    groups = ((0, 1), (1, 3))
    fleft = [[fresh() for _ in range(8)] for _ in groups]
    fright = [[fresh() for _ in range(7)] for _ in groups]

    def fblk(g, zz):
        lo, hi = groups[g]
        return ffw.at[lo:hi, :, pl.ds(pl.multiple_of(zz * 128, 128), 128)]

    def f_send(g, zz, sem, where):
        copy_to(fblk(g, zz), fblk(g, zz), fsend.at[g], sem, where).start()

    def serve_f(g, s):
        if s == 0:
            f_send(g, z, fleft[g][0], at(zz=zr))
            f_send(g, z, fright[g][0], at(zz=zl))
            return
        zz = (z + Z - s) % Z
        copy_to(fblk(g, zz), fblk(g, zz), fsend.at[g], fleft[g][s - 1], at(zz=zr)).wait_recv()
        if s < 8:
            f_send(g, zz, fleft[g][s], at(zz=zr))
        if s <= 7:
            zz = (z + s) % Z
            copy_to(fblk(g, zz), fblk(g, zz), fsend.at[g], fright[g][s - 1], at(zz=zl)).wait_recv()
            if s < 7:
                f_send(g, zz, fright[g][s], at(zz=zl))

    serve_w(0)

    def to_sibling(ref, sem):
        return send(ref, ref, sem, at(cc=o))

    tok_ring = Ring4(
        lambda j, half=None: xt.at[c, j, (slice(0, 272), slice(0, 144), slice(144, 272))[0 if half is None else half + 1], :],
        x, xm, xp, at(xx=xm), at(xx=xp),
    )
    tok_ring.start()
    tok_sib = [to_sibling(xt.at[c, x], fresh())]
    a2a_copies = []
    for yy in (yp, y2, ym):
        a2a_copies.append(
            send(slab.at[pl.ds(pl.multiple_of(yy * HID, 16), HID), :], a2a.at[y], fresh(), at(yy=yy))
        )
    serve_w(1)
    tok_ring.relay()
    tok_sib += [to_sibling(xt.at[c, xm], fresh()), to_sibling(xt.at[c, xp], fresh())]
    relay_y(0)
    for copy in a2a_copies:
        copy.wait_recv()

    pick = jnp.zeros((HID, 384), F32)
    ln, col = iota((128, 384), 0), iota((128, 384), 1)
    same = (ln // 32 == col // 128) & (ln % 32 == col % 32)
    own = slab[pl.ds(pl.multiple_of(y * HID, 16), HID), :]
    for yy in range(Y):
        chosen = (same & ((col % 128) // 32 == yy)).astype(BF16)
        pick = pick + dot(jnp.where(yy == y, own, a2a[yy]), chosen)
    zlane = pl.ds(pl.multiple_of(z * 128, 128), 128)
    for p in range(3):
        ffw[p, :, zlane] = pick[:, p * 128 : (p + 1) * 128].astype(BF16)

    serve_w(2)
    relay_y(1)
    serve_f(0, 0)
    tok_ring.finish()
    tok_sib.append(to_sibling(xt.at[c, xo], fresh()))
    serve_w(3)
    relay_y(2)
    serve_f(0, 1)
    serve_f(1, 0)
    for copy in tok_sib:
        copy.wait_recv()

    total = jnp.zeros((SEQ, 1), F32)
    for t in range(8):
        v = xt[t % 2, t // 2, 0:256, :].astype(F32)
        total = total + jnp.sum(v * v, axis=1, keepdims=True)
    scale = lax.rsqrt(total * (1.0 / D) + EPS)
    for t in range(8):
        v = xt[t % 2, t // 2, 0:256, :].astype(F32)
        g = xt[t % 2, t // 2, 256:257, :].astype(F32)
        xn[:, t * 256 : (t + 1) * 256] = (v * scale * g).astype(BF16)

    for s in range(4, 9):
        serve_w(s)
        relay_y(s - 1)
        serve_f(0, s - 2)
    relay_y(8)
    wait_bytes(wq.at[0 : 7 * 32], yshare.at[0])
    wait_bytes(wq.at[0 : 9 * 32], yshare.at[1])
    wait_bytes(wq.at[0 : 9 * 32], yshare.at[2])
    wait_bytes(wq.at[0 : 7 * 32], yshare.at[3])

    def wo_src(t):
        return wq.at[pl.ds(pl.multiple_of(t * 256, 256), 256), 384:512]

    wo_copies = []
    for xx, cc in [(xx, cc) for xx in (x, xp, xo, xm) for cc in (c, o)][1:]:
        wo_copies.append(send(wo_src(xx * C + cc), wo.at[c, x], fresh(), at(xx=xx, cc=cc)))
    wo[c, x] = wq[pl.ds(pl.multiple_of(tp * 256, 256), 256), 384:512]

    proj = dot(xn[...], wq[:, 0:384])
    serve_f(0, 7)
    serve_f(0, 8)
    serve_f(1, 1)

    qk = proj[:, 0:128]
    lane = iota((SEQ, 128), 1)
    swapped = jnp.where(lane % 64 < 32, pltpu.roll(qk, 96, 1), pltpu.roll(qk, 32, 1))
    turned_qk = qk * cos[...] + swapped * sin[...]
    query = jnp.where(lane < 64, turned_qk, 0.0).astype(BF16)
    key = pltpu.roll(turned_qk, 64, 1).astype(BF16)
    value = proj[:, 128:256].astype(BF16)
    later, earlier = iota((SEQ, SEQ), 0), iota((SEQ, SEQ), 1)
    n0 = jnp.minimum(later, BLK - 1) - jnp.minimum(earlier, BLK - 1)
    n1 = jnp.maximum(later, BLK - 1) - jnp.maximum(earlier, BLK - 1)
    rate = rates[0]
    power = n0.astype(F32) * (-rate * scales[0]) + n1.astype(F32) * (-rate * scales[1])
    causal = later >= earlier
    inside = jnp.where(causal, jnp.exp(jnp.where(causal, power, 0.0)), 0.0)
    scores = dot_nt(query, key) * inside
    high = scores.astype(BF16)
    low = (scores - high.astype(F32)).astype(BF16)
    ret = dot(high, value) + dot(low, value)
    ret = ret * lax.rsqrt(jnp.mean(ret * ret, axis=1, keepdims=True) + EPS)
    g = proj[:, 256:384]
    gat[c, x] = (ret * (g * jax.nn.sigmoid(g))).astype(BF16)
    serve_f(1, 2)
    gat_ring = Ring4(
        lambda j, half=None: gat.at[c, j, (slice(0, 256), slice(0, 128), slice(128, 256))[0 if half is None else half + 1], :],
        x, xm, xp, at(xx=xm), at(xx=xp),
    )
    gat_ring.start()
    gat_sib = [to_sibling(gat.at[c, x], fresh())]
    gat_ring.relay()
    gat_sib += [to_sibling(gat.at[c, xm], fresh()), to_sibling(gat.at[c, xp], fresh())]
    serve_f(1, 3)
    gat_ring.finish()
    gat_sib.append(to_sibling(gat.at[c, xo], fresh()))
    for copy in wo_copies:
        copy.wait_recv()
    for copy in gat_sib:
        copy.wait_recv()
    mix = jnp.zeros((SEQ, 256), F32)
    for t in range(8):
        term = dot_nt(gat[t % 2, t // 2], wo[t % 2, t // 2])
        mix = mix + term.astype(BF16).astype(F32)
    resid = (tok[...].astype(F32) + mix).astype(BF16)
    res[...] = resid
    x2[c, y, x] = resid
    serve_f(1, 4)

    A, B = slice(0, 128), slice(128, 256)

    def pair(half):
        return slice(0, 4) if half is None else slice(2 * half, 2 * half + 2)

    def rows(base, half):
        return slice(base, base + 128) if half is None else slice(base + 64 * half, base + 64 * half + 64)

    toy, tox = (at(yy=ym), at(yy=yp)), (at(xx=xm), at(xx=xp))
    ring_a1 = Ring4(lambda j, half=None: x2.at[c, y, j, rows(0, half), :], x, xm, xp, *tox)
    ring_b1 = Ring4(lambda j, half=None: x2.at[c, j, x, rows(128, half), :], y, ym, yp, *toy)
    ring_a2 = Ring4(lambda j, half=None: x2.at[c, j, pair(half), A, :], y, ym, yp, *toy)
    ring_b2 = Ring4(lambda j, half=None: x2.at[c, pair(half), j, B, :], x, xm, xp, *tox)
    ring_a1.start()
    ring_b1.start()
    ring_a1.relay()
    ring_b1.relay()
    serve_f(1, 5)
    ring_a1.finish()
    ring_a2.start()
    ring_b1.finish()
    ring_b2.start()
    x2_sib = [to_sibling(x2.at[c, y, :, A, :], fresh()), to_sibling(x2.at[c, :, x, B, :], fresh())]
    serve_f(1, 6)
    ring_a2.relay()
    ring_b2.relay()
    for yy, xx in ((ym, xm), (yp, xp)):
        x2_sib += [to_sibling(x2.at[c, yy, :, A, :], fresh()), to_sibling(x2.at[c, :, xx, B, :], fresh())]
    serve_f(1, 7)
    serve_f(1, 8)
    ring_a2.finish()
    ring_b2.finish()
    x2_sib += [to_sibling(x2.at[c, y2, :, A, :], fresh()), to_sibling(x2.at[c, :, xo, B, :], fresh())]
    for copy in x2_sib:
        copy.wait_recv()

    part_sem = [fresh() for _ in range(Y)]
    part_copies = []
    for s in range(Y):
        total = jnp.zeros((SEQ, 1), F32)
        for t in range(8):
            v = x2[t % 2, s, t // 2].astype(F32)
            total = total + jnp.sum(v * v, axis=1, keepdims=True)
        scale = lax.rsqrt(total * (1.0 / D) + EPS)
        for t in range(8):
            v = x2[t % 2, s, t // 2].astype(F32)
            g = xt[t % 2, t // 2, 264:265, :].astype(F32)
            xn[:, t * 256 : (t + 1) * 256] = (v * scale * g).astype(BF16)
        gate = dot_nt(xn[...], ffw[0])
        up = dot_nt(xn[...], ffw[1])
        hidden = (gate * jax.nn.sigmoid(gate) * up).astype(BF16)
        for cc in (o, c):
            for xx in range(X):
                lanes = pl.ds(pl.multiple_of((xx * C + cc) * 256, 256), 256)
                part[cc, s, xx] = dot(hidden, ffw[2, :, lanes]).astype(BF16)
            if cc is o:
                part_copies.append(send(part.at[o, s], sib.at[s], part_sem[s], at(cc=o)))
    for s in range(Y):
        part_copies[s].wait_recv()
        part[c, s] = part[c, s] + sib[s]

    class Sum4:
        def __init__(self, slab_of, first, second, me, prev, nxt, opp, to_prev, to_next):
            self.slab, self.first, self.second = slab_of, first, second
            self.me, self.prev, self.nxt, self.opp = me, prev, nxt, opp
            self.to_prev, self.to_next = to_prev, to_next
            self.sems = [fresh() for _ in range(4)]

        def start(self):
            self.a = send(self.slab(self.opp, 0), self.first.at[0], self.sems[0], self.to_next)
            self.b = send(self.slab(self.opp, 1), self.first.at[1], self.sems[1], self.to_prev)

        def middle(self):
            self.a.wait_recv()
            ref = self.slab(self.nxt, 0)
            ref[...] = ref[...] + self.first[0]
            self.b.wait_recv()
            ref = self.slab(self.prev, 1)
            ref[...] = ref[...] + self.first[1]
            self.d = send(self.slab(self.nxt), self.second.at[0], self.sems[2], self.to_next)
            self.e = send(self.slab(self.prev), self.second.at[1], self.sems[3], self.to_prev)

        def finish(self):
            self.d.wait_recv()
            self.e.wait_recv()

    sum_a1 = Sum4(lambda j, half=None: part.at[c, j, pair(half), A, :], r1.at[0], r2.at[0], y, ym, yp, y2, *toy)
    sum_b1 = Sum4(lambda j, half=None: part.at[c, pair(half), j, B, :], r1.at[1], r2.at[1], x, xm, xp, xo, *tox)
    sum_a2 = Sum4(lambda j, half=None: part.at[c, y, j, rows(0, half), :], r3.at[0], r4.at[0], x, xm, xp, xo, *tox)
    sum_b2 = Sum4(lambda j, half=None: part.at[c, j, x, rows(128, half), :], r3.at[1], r4.at[1], y, ym, yp, y2, *toy)
    sum_a1.start()
    sum_b1.start()
    sum_a1.middle()
    sum_b1.middle()
    sum_a1.finish()
    for xx in range(X):
        mine = part[c, y, xx, A, :].astype(F32) + r2[0, 0, xx].astype(F32) + r2[0, 1, xx].astype(F32)
        part[c, y, xx, A, :] = mine.astype(BF16)
    sum_a2.start()
    sum_b1.finish()
    for yy in range(Y):
        mine = part[c, yy, x, B, :].astype(F32) + r2[1, 0, yy].astype(F32) + r2[1, 1, yy].astype(F32)
        part[c, yy, x, B, :] = mine.astype(BF16)
    sum_b2.start()
    sum_a2.middle()
    sum_b2.middle()
    sum_a2.finish()
    sum_b2.finish()
    ffn = jnp.concatenate(
        [r4[h, 0].astype(F32) + r4[h, 1].astype(F32) for h in range(2)], axis=0
    ) + part[c, y, x].astype(F32)
    total = res[...].astype(F32) + ffn

    squares = jnp.sum(total * total, axis=1, keepdims=True)
    turned = jnp.broadcast_to(squares, (SEQ, 128)).T
    stat[...] = turned[0:8, :]
    stat_copies = []
    for xx, cc in [(xx, cc) for xx in (x, xp, xo, xm) for cc in (c, o)][1:]:
        stat_copies.append(send(stat, stats.at[c, x], fresh(), at(xx=xx, cc=cc)))
    stats[c, x] = turned[0:8, :]
    for copy in stat_copies:
        copy.wait_recv()
    summed = stats[0, 0]
    for t in range(1, 8):
        summed = summed + stats[t % 2, t // 2]
    across = jnp.concatenate([summed] * 16, axis=0).T
    scale = lax.rsqrt(across * (1.0 / D) + EPS)
    out[:, 0:128] = (total[:, 0:128] * scale * fin[:, 0:128].astype(F32)).astype(BF16)
    out[:, 128:256] = (total[:, 128:256] * scale * fin[:, 128:256].astype(F32)).astype(BF16)

    for copy in pending:
        copy.wait_send()
    wait_bytes(wq.at[0 : 15 * 32], zsend)
    wait_bytes(wq.at[0 : 48 * 32], ysend)
    for g, (lo, hi) in enumerate(groups):
        wait_bytes(ffw.at[lo:hi, :, 0 : 15 * 128], fsend.at[g])
    assert used[0] <= N_SEND and used[1] <= N_RECV, used


def tables():
    half = DK // 2
    inverse = THETA ** (-np.arange(half, dtype=np.float64) / half)
    angle = np.arange(SEQ, dtype=np.float64)[:, None] * inverse
    cosine, sine = np.cos(angle), np.sin(angle)
    c1 = np.concatenate([cosine, cosine], axis=1)
    s1 = np.concatenate([-sine, sine], axis=1)
    k = DK ** (-0.5)
    return (
        np.concatenate([c1, c1 * k], axis=1).astype(np.float32),
        np.concatenate([s1, s1 * k], axis=1).astype(np.float32),
    )


def body(tokens, mix_gain, qw, kw, vw, gw, ow, rates, scales, ffn_gain, ffg, ffu, ffd, fin):
    cos, sin = tables()
    vmem = pl.BlockSpec(memory_space=pltpu.VMEM)
    smem = pl.BlockSpec(memory_space=pltpu.SMEM)
    return pl.pallas_call(
        kernel,
        name="layer",
        out_shape=jax.ShapeDtypeStruct((SEQ, 256), BF16),
        in_specs=[vmem] * 7 + [smem] * 2 + [vmem] * 7,
        out_specs=vmem,
        scratch_shapes=[
            pltpu.VMEM((D, 512), BF16),
            pltpu.VMEM((704, 128), BF16),
            pltpu.VMEM((Y, HID, 128), BF16),
            pltpu.VMEM((3, HID, D), BF16),
            pltpu.VMEM((C, X, 272, 256), BF16),
            pltpu.VMEM((SEQ, D), BF16),
            pltpu.VMEM((C, X, 256, 128), BF16),
            pltpu.VMEM((C, X, 256, 128), BF16),
            pltpu.VMEM((SEQ, 256), BF16),
            pltpu.VMEM((C, Y, X, 256, 256), BF16),
            pltpu.VMEM((C, Y, X, 256, 256), BF16),
            pltpu.VMEM((Y, X, 256, 256), BF16),
            pltpu.VMEM((2, 2, 2, 128, 256), BF16),
            pltpu.VMEM((2, 2, 4, 128, 256), BF16),
            pltpu.VMEM((2, 2, 64, 256), BF16),
            pltpu.VMEM((2, 2, 128, 256), BF16),
            pltpu.VMEM((8, SEQ), F32),
            pltpu.VMEM((C, X, 8, SEQ), F32),
            pltpu.SemaphoreType.DMA((N_SEND,)),
            pltpu.SemaphoreType.DMA((N_RECV,)),
            pltpu.SemaphoreType.DMA,
            pltpu.SemaphoreType.DMA,
            pltpu.SemaphoreType.DMA((2,)),
            pltpu.SemaphoreType.DMA((4,)),
        ],
        compiler_params=pltpu.CompilerParams(
            collective_id=0, has_side_effects=True, vmem_limit_bytes=60 * 1024 * 1024
        ),
    )(
        tokens, mix_gain.reshape(1, 256), qw, kw, vw, gw, ow, rates, scales,
        ffn_gain.reshape(1, 256), ffg, ffu, ffd, fin.reshape(1, 256),
        jnp.asarray(cos), jnp.asarray(sin),
    )


def solution(mesh):
    return jax.shard_map(
        body,
        mesh=mesh,
        in_specs=(
            P("fs", "tp"), P("tp"), P("fs", "tp"), P("fs", "tp"), P("fs", "tp"), P("fs", "tp"),
            P("tp", "fs"), P("tp"), P("fs"), P("tp"), P("fs", "tp"), P("fs", "tp"), P("tp", "fs"), P("tp"),
        ),
        out_specs=P("fs", "tp"),
        check_vma=False,
    )
```

time: 517 us -> 126 us (0.24)
  waiting for transfers between devices: 349 us -> 0 us
  Pallas kernels: 0 us -> 119 us
  blocking collectives: 81 us -> 0 us
  starting transfers between devices: 33.6 us -> 0 us
  matrix products: 19.1 us -> 0 us
  between operations: 14.1 us -> 0.7 us
  other arithmetic: 12 us -> 0 us
    all_gather x5 -> x0, waiting for transfers between devices: 335 us -> none  [the longest x2 252 us: sent_together(): filled = lax.all_gather(both, axis, axis=dim, tiled=True)]
    pallas_call x0 -> x1, Pallas kernels: none -> 119 us  [body(): pl.pallas_call(kernel, name='layer', out_shape=jax.ShapeDtypeStruct((SEQ,...]
    all_gather x3 -> x0, blocking collectives: 52.5 us -> none  [gathered_by_axis(): filled = lax.all_gather(filled, axes[number], axis=dim, tiled=True)]
    all_to_all x3 -> x0, starting transfers between devices: 33.5 us -> none  [the longest x2 19.4 us: copy_for_each(): lax.all_to_all(jnp.broadcast_to(shard[None], (size, *shard.shape)), axis,...]
    all_to_all x1 -> x0, blocking collectives: 28.6 us -> none  [sent_and_summed(): tiles = lax.all_to_all(in_blocks(shard, dim, size), axis, 0, 0, tiled=True)]
    dot_general x11 -> x0, matrix products: 19.1 us -> none  [the longest x1 7.24 us: body(): jnp.dot(hidden, gathered_by_axis(ff_down, FS, 1), preferred_element_type=...]
    all_to_all x3 -> x0, waiting for transfers between devices: 14 us -> none  [the longest x2 14 us: copy_for_each(): lax.all_to_all(jnp.broadcast_to(shard[None], (size, *shard.shape)), axis,...]
  transfers between devices with their start and end apart: 8 -> 0, of which waited for: 6 -> 0; matrix products, arithmetic and copies ran while one was open for 5% -> 0% of each run, Pallas kernels for 0% -> 0%
where the time goes in v1:
time: 126 us
  Pallas kernels  119 us (94%)
  local copies, waits for them, and re-layouts  6.46 us (5%)
    pallas_call x1, Pallas kernels, body(): pl.pallas_call(kernel, name='layer', out_shape=jax.ShapeDtypeStruct((SEQ,...  119 us
    unnamed x9, local copies, waits for them, and re-layouts  4.79 us

profile of v1, /device:TPU:1, one launch (start us, length us, event | category | flops | bytes accessed | tf_op | source)
XLA Modules:
  0.0 125.8 jit_solution(3370670107456995225)
XLA Ops:
  0.0 0.0 copy-start
  0.7 0.0 copy-done
  0.7 0.0 copy-start.1
  0.7 0.5 reshape.9.mix_gain
  1.2 0.1 copy-done.1
  1.3 0.0 copy-start.2
  1.3 0.5 reshape.10.ffn_gain
  1.9 0.1 copy-done.2
  2.0 0.6 reshape.11.fin
  2.6 1.4 %copy.17.ow = bf16[128,32]{1,0:T(8,128)(2,1)} copy(bf16[128,32]{0,1:T(8,128)(2,1)} %param.22) | data formatting | bytes 16384 | tf_op args[6]
  4.0 1.6 %copy.18.ffd = bf16[704,32]{1,0:T(8,128)(2,1)} copy(bf16[704,32]{0,1:T(8,128)(2,1)} %param.28) | data formatting | bytes 90112 | tf_op args[12]
  5.6 118.6 %layer.1 = bf16[256,256]{1,0:T(8,128)(2,1)} custom-call(bf16[256,256]{1,0:T(8,128)(2,1)} %tok.1, bf16[1,256]{1,0:T(2,128)(2,1)} %reshape.9.mix_gain, bf16[32,64]{1,0:T(8,128)(2,1)} %qw.1, bf16[32,64]{1,0:T(8,128)(2,1)} %kw.1, bf16[32,128]{1,0:T(8,128)(2,1)} %vw.1, bf16[32,128]{1,0:T(8,128)(2,1)} %gw.1, bf16[128,32]{1,0:T(8,128)(2,1)} %copy.17.ow, ...), custom_call_target="tpu_custom_call" | custom-call | tf_op jit(solution)/shard_map/layer/pallas_call | solution.py:481
  124.2 1.6 %copy.21 = bf16[256,256]{1,0:T(8,128)(2,1)} copy(bf16[256,256]{1,0:T(8,128)(2,1)} %layer.1) | data formatting | bytes 262144
Async XLA Ops:
  0.0 0.7 copy-start
  0.7 0.7 copy-start.1
  1.3 0.7 copy-start.2
